TPU v7x, 512 devices: a whole 4x8x8 slice. The times are simulated.
512 devices in a mesh: sp: 64 (over z, y), tp: 8 (over x, core).
Axes of the slice: x: 4, y: 8, z: 8, core: 2. Of those that a mesh axis runs over, the one named last changes fastest.
Arguments:
- queries: bfloat16 [32768, 2048], P('sp', 'tp'), may hold values from -14 to 14
- key_states: bfloat16 [32768, 512], P('sp', 'tp'), may hold values from -14 to 14
- value_states: bfloat16 [32768, 512], P('sp', 'tp'), may hold values from -6 to 6
- sink_logits: float32 [32], P('tp'), may hold values from 0 to 5
- out_weight: bfloat16 [2048, 2048], P('tp'), may hold values from -0.125 to 0.125
- residual: bfloat16 [32768, 2048], P(('sp', 'tp')), may hold values from -6 to 6
- gain_attn: float32 [2048], replicated, may hold values from 0.1 to 1.9
- gain_before: float32 [2048], replicated, may hold values from 0.1 to 1.9
- gain_after: float32 [2048], replicated, may hold values from 0.1 to 1.9
- gate_weight: bfloat16 [2048, 5632], P('sp', 'tp'), may hold values from -0.125 to 0.125
- value_weight: bfloat16 [2048, 5632], P('sp', 'tp'), may hold values from -0.125 to 0.125
- gate_taps: float32 [3, 5632], P(None, 'tp'), may hold values from -3 to 3
- value_taps: float32 [3, 5632], P(None, 'tp'), may hold values from -3 to 3
- down_weight: bfloat16 [5632, 2048], P('tp', 'sp'), may hold values from -0.078125 to 0.078125
Outputs:
- layer_out: bfloat16 [32768, 2048], P(('sp', 'tp'))
All inputs are finite; a program needn't handle non-finite values.
Results may differ from a plain program's by a relative error of at most 0.018.
Values may be sent and summed in bfloat16 or wider, within the bound.
A program may use at most 64 MiB of HBM per device.

v0:
```python
import jax
import jax.numpy as jnp
from jax import lax
from jax.sharding import PartitionSpec as P

HD = 64
WINDOW = 128
NEG_FILL = -1e30


def passed_along(block, axis, distance):
    devices = range(lax.axis_size(axis))
    route = [(i - distance, i) for i in devices if i - distance in devices]
    return lax.ppermute(block, axis, route)


def in_blocks(shard, dim, peers):
    before, after = (shard.shape[:dim], shard.shape[dim + 1 :])
    return jnp.moveaxis(shard.reshape(*before, peers, -1, *after), dim, 0)


def sum_at_owner(shard, axis, dim):
    peers = lax.axis_size(axis)
    pieces = lax.all_to_all(in_blocks(shard, dim, peers), axis, 0, 0, tiled=True)
    return jnp.sum(pieces.astype(jnp.float32), axis=0)


def in_order(pieces, dim):
    pieces = jnp.moveaxis(pieces, 0, dim)
    lengths = pieces.shape
    return pieces.reshape(*lengths[:dim], lengths[dim] * lengths[dim + 1], *lengths[dim + 2 :])


def sent_to_all(shard, axis):
    copies = jnp.broadcast_to(shard, (lax.axis_size(axis), *shard.shape))
    return lax.all_to_all(copies, axis, split_axis=0, concat_axis=0, tiled=True)


def gather_directly(shard, axis, dim):
    return in_order(sent_to_all(shard, axis), dim)


def in_one_piece(arrays, axis, dim, along):
    widths = [a.shape[along] for a in arrays]
    both = jnp.concatenate(arrays, axis=along)
    filled = lax.all_gather(both, axis, axis=dim, tiled=True)
    return tuple(jnp.split(filled, [sum(widths[:k]) for k in range(1, len(widths))], axis=along))


def rms_scale(matrix):
    return matrix * lax.rsqrt(jnp.mean(matrix * matrix, axis=-1, keepdims=True) + 1e-06)


def attention_local(queries, key_states, value_states, sink_logits):
    length = queries.shape[0]
    blocks = length // WINDOW
    kv_local = key_states.shape[1] // HD
    grouping = queries.shape[1] // key_states.shape[1]
    earlier_keys, earlier_values = passed_along(
        (key_states[length - WINDOW :], value_states[length - WINDOW :]), "sp", 1
    )
    keys_ext = jnp.concatenate([earlier_keys, key_states], axis=0).reshape(
        blocks + 1, WINDOW, kv_local, HD
    )
    values_ext = jnp.concatenate([earlier_values, value_states], axis=0).reshape(
        blocks + 1, WINDOW, kv_local, HD
    )
    key_blocks = jnp.concatenate([keys_ext[:-1], keys_ext[1:]], axis=1)
    value_blocks = jnp.concatenate([values_ext[:-1], values_ext[1:]], axis=1)
    query_blocks = queries.reshape(blocks, WINDOW, kv_local, grouping, HD)
    offset = lax.axis_index("sp") * length
    qpos = (offset + jnp.arange(length, dtype=jnp.int32)).reshape(blocks, WINDOW)
    kpos = jnp.concatenate([qpos - WINDOW, qpos], axis=1)
    visible = (
        (kpos[:, None, :] <= qpos[:, :, None])
        & (qpos[:, :, None] - kpos[:, None, :] < WINDOW)
        & (kpos[:, None, :] >= 0)
    )
    scores = jnp.einsum(
        "nqhgd,nkhd->nhgqk", query_blocks, key_blocks, preferred_element_type=jnp.float32
    ) * HD ** (-0.5)
    scores = jnp.where(visible[:, None, None], scores, NEG_FILL)
    sink_col = sink_logits.reshape(kv_local, grouping)[None, :, :, None]
    top = jnp.maximum(jnp.max(scores, axis=-1), sink_col)
    expo = jnp.exp(scores - top[..., None])
    total = jnp.sum(expo, axis=-1) + jnp.exp(sink_col - top)
    probs = (expo / total[..., None]).astype(jnp.bfloat16)
    result = jnp.einsum(
        "nhgqk,nkhd->nqhgd", probs, value_blocks, preferred_element_type=jnp.float32
    )
    return result.astype(jnp.bfloat16).reshape(length, queries.shape[1])


def causal_local(upward, earlier, kernel):
    length = upward.shape[0]
    padded = jnp.concatenate([earlier, upward], axis=0).astype(jnp.float32)
    result = jnp.zeros(upward.shape, jnp.float32)
    for tap_index in range(kernel.shape[0]):
        result = result + kernel[tap_index][None, :] * padded[tap_index : tap_index + length]
    return result


def on_device(
    queries,
    key_states,
    value_states,
    sink_logits,
    out_weight,
    residual,
    gain_attn,
    gain_before,
    gain_after,
    gate_weight,
    value_weight,
    gate_taps,
    value_taps,
    down_weight,
):
    length = queries.shape[0]
    attended = attention_local(queries, key_states, value_states, sink_logits)
    selected = attended
    attn_proj = sum_at_owner(
        jnp.dot(selected, out_weight, preferred_element_type=jnp.float32).astype(jnp.bfloat16),
        "tp",
        0,
    )
    middle = residual.astype(jnp.float32) + rms_scale(attn_proj) * gain_attn
    normed = (rms_scale(middle) * gain_before).astype(jnp.bfloat16)
    whole_rows = gather_directly(normed, "tp", 0)
    gate_full, value_full = in_one_piece((gate_weight, value_weight), "sp", 0, 1)
    gate_up = jnp.dot(whole_rows, gate_full, preferred_element_type=jnp.float32).astype(
        jnp.bfloat16
    )
    value_up = jnp.dot(whole_rows, value_full, preferred_element_type=jnp.float32).astype(
        jnp.bfloat16
    )
    reach = gate_taps.shape[0] - 1
    gate_before, value_before = passed_along(
        (gate_up[length - reach :], value_up[length - reach :]), "sp", 1
    )
    gate_conv = causal_local(gate_up, gate_before, gate_taps)
    value_conv = causal_local(value_up, value_before, value_taps)
    hidden = (jax.nn.silu(gate_conv) * value_conv).astype(jnp.bfloat16)
    down_whole = lax.all_gather(down_weight, "sp", axis=1, tiled=True)
    selected = hidden
    down = sum_at_owner(
        jnp.dot(selected, down_whole, preferred_element_type=jnp.float32).astype(jnp.bfloat16),
        "tp",
        0,
    )
    return (middle + rms_scale(down) * gain_after).astype(jnp.bfloat16)


def solution(mesh):
    in_specs = (
        P("sp", "tp"),
        P("sp", "tp"),
        P("sp", "tp"),
        P("tp"),
        P("tp", None),
        P(("sp", "tp"), None),
        P(),
        P(),
        P(),
        P("sp", "tp"),
        P("sp", "tp"),
        P(None, "tp"),
        P(None, "tp"),
        P("tp", "sp"),
    )
    out_specs = P(("sp", "tp"), None)
    return jax.shard_map(
        on_device, mesh=mesh, in_specs=in_specs, out_specs=out_specs, check_vma=False
    )
```

profile of v0, /device:TPU:1, one launch (start us, length us, event | category | flops | bytes accessed | tf_op | source)
XLA Modules:
  0.0 238.2 jit_solution(13050096968348563992)
XLA Ops:
  6.5 0.0 copy-start
  6.5 0.0 all-gather.3.cloned.1.call-start
  6.5 1.6 pad_maximum_fusion
  8.2 0.0 all-gather.3.cloned.1.call-update
  8.2 0.7 slice.72
  8.9 4.0 %collective-permute-start.1 = (bf16[128,64]{0,1:T(8,128)(2,1)S(1)}, bf16[128,64]{0,1:T(8,128)(2,1)S(1)}, u32[]{:S(2)}, u32[]{:S(2)}) collective-permute-start(bf16[128,64]{0,1:T(8,128)(2,1)S(1)} %slice.72), channel_id=1, source_target_pairs={{0,8},{8,16},{16,24},{24,32},{32,40},{40,48},{48,56},{56,64},{64,7... | collective-permute-start | bytes 49160 | tf_op jit(solution)/shard_map/ppermute | solution.py:14
  13.0 0.7 slice.68
  13.7 3.2 %collective-permute-start = (bf16[128,64]{0,1:T(8,128)(2,1)S(1)}, bf16[128,64]{0,1:T(8,128)(2,1)S(1)}, u32[]{:S(2)}, u32[]{:S(2)}) collective-permute-start(bf16[128,64]{0,1:T(8,128)(2,1)S(1)} %slice.68), channel_id=1, source_target_pairs={{0,8},{8,16},{16,24},{24,32},{32,40},{40,48},{48,56},{56,64},{64,7... | collective-permute-start | bytes 49160 | tf_op jit(solution)/shard_map/ppermute | solution.py:14
  16.9 0.3 fusion.29
  17.3 0.9 slice.75
  18.1 0.9 slice.71
  19.0 1.2 reshape.136
  20.2 0.0 copy-start.8
  20.3 0.0 collective-permute-done.1
  20.3 0.8 pad_maximum_fusion.1
  21.2 0.0 collective-permute-done
  21.2 0.0 copy-done.2
  21.2 0.5 fusion.39
  21.8 0.0 copy-done.8
  21.8 0.1 broadcast_maximum_fusion
  21.9 0.3 fusion.4
  22.2 0.1 exponential_add_fusion
  22.3 0.5 fusion.17
  22.8 0.2 copy.24
  23.0 0.0 copy-done
  23.0 2.1 convolution_convert_fusion
  25.1 6.4 %all-to-all-start = ((bf16[8,64,2048]{2,1,0:T(8,128)(2,1)}), bf16[8,64,2048]{2,1,0:T(8,128)(2,1)}, u32[]{:S(2)}, u32[]{:S(2)}) async-start(bf16[8,64,2048]{2,1,0:T(8,128)(2,1)} %bitcast.11), calls=%async_computation | async-start | bytes 4194304 | tf_op jit(solution)/shard_map/all_to_all | solution.py:24
  31.5 0.0 copy-start.1
  31.5 0.0 copy-start.3
  31.5 0.0 all-gather.5.cloned.1.call-start
  31.6 0.7 all-gather.5.cloned.1.call-update
  32.3 25.6 %all-to-all-done = bf16[8,64,2048]{2,1,0:T(8,128)(2,1)} async-done(((bf16[8,64,2048]{2,1,0:T(8,128)(2,1)}), bf16[8,64,2048]{2,1,0:T(8,128)(2,1)}, u32[]{:S(2)}, u32[]{:S(2)}) %all-to-all-start) | async-done | bytes 2097184 | tf_op jit(solution)/shard_map/all_to_all | solution.py:24
  57.9 2.0 convert_reduce_fusion.1
  59.9 0.1 multiply_reduce_fusion.2
  60.0 0.0 copy-done.1
  60.0 0.0 copy-done.3
  60.0 0.3 multiply_reduce_fusion.1
  60.3 0.0 copy-done.4
  60.3 0.2 multiply_convert_fusion
  60.5 1.6 broadcast_in_dim.16
  62.1 5.3 %all-to-all-start.1 = ((bf16[8,64,2048]{2,1,0:T(8,128)(2,1)}), bf16[8,64,2048]{2,1,0:T(8,128)(2,1)}, u32[]{:S(2)}, u32[]{:S(2)}) async-start(bf16[8,64,2048]{2,1,0:T(8,128)(2,1)} %broadcast_in_dim.16), calls=%async_computation.1 | async-start | bytes 4194304 | tf_op jit(solution)/shard_map/all_to_all | solution.py:36
  67.5 0.0 copy-done.6
  67.5 0.0 copy-done.7
  67.5 0.1 slice_reduce_fusion.2
  67.6 26.3 %all-to-all-done.1 = bf16[8,64,2048]{2,1,0:T(8,128)(2,1)} async-done(((bf16[8,64,2048]{2,1,0:T(8,128)(2,1)}), bf16[8,64,2048]{2,1,0:T(8,128)(2,1)}, u32[]{:S(2)}, u32[]{:S(2)}) %all-to-all-start.1) | async-done | bytes 2097184 | tf_op jit(solution)/shard_map/all_to_all | solution.py:36
  93.8 8.4 %all-gather.3.cloned.1.call-done = bf16[2048,1408]{1,0:T(8,128)(2,1)} async-done(((bf16[32,1408]{1,0:T(8,128)(2,1)}), bf16[2048,1408]{1,0:T(8,128)(2,1)}) %all-gather.3.cloned.1.call-update) | async-done | bytes 5767184 | tf_op jit(solution)/shard_map/all_gather | solution.py:46
  102.2 4.4 %fusion.11 = bf16[512,704]{0,1:T(8,128)(2,1)S(1)} fusion(bf16[512,2048]{1,0:T(8,128)(2,1)} %bitcast.12, bf16[2048,1408]{1,0:T(8,128)(2,1)} %all-gather.3.cloned.1.call-done), kind=kOutput, calls=%fused_computation.24 | convolution fusion | flops 1476755456 | bytes 5963776 | tf_op jit(solution)/shard_map/dot_general | solution.py:131
  106.6 0.1 slice.90
  106.7 2.7 %collective-permute-start.2 = (bf16[2,704]{0,1:T(8,128)(2,1)S(1)}, bf16[2,704]{0,1:T(8,128)(2,1)S(1)}, u32[]{:S(2)}, u32[]{:S(2)}) collective-permute-start(bf16[2,704]{0,1:T(8,128)(2,1)S(1)} %slice.90), channel_id=1, source_target_pairs={{0,8},{8,16},{16,24},{24,32},{32,40},{40,48},{48,56},{56,64},{64,7... | collective-permute-start | bytes 8456 | tf_op jit(solution)/shard_map/ppermute | solution.py:14
  109.4 0.0 copy-done.9
  109.4 4.5 %fusion.14 = bf16[512,704]{0,1:T(8,128)(2,1)S(1)} fusion(bf16[512,2048]{1,0:T(8,128)(2,1)} %bitcast.12, bf16[2048,1408]{1,0:T(8,128)(2,1)S(1)} %copy-done.9), kind=kOutput, calls=%fused_computation.25 | convolution fusion | flops 1476755456 | bytes 5963776 | tf_op jit(solution)/shard_map/dot_general | solution.py:134
  113.9 0.1 slice.94
  114.0 3.7 %collective-permute-start.3 = (bf16[2,704]{0,1:T(8,128)(2,1)S(1)}, bf16[2,704]{0,1:T(8,128)(2,1)S(1)}, u32[]{:S(2)}, u32[]{:S(2)}) collective-permute-start(bf16[2,704]{0,1:T(8,128)(2,1)S(1)} %slice.94), channel_id=1, source_target_pairs={{0,8},{8,16},{16,24},{24,32},{32,40},{40,48},{48,56},{56,64},{64,7... | collective-permute-start | bytes 8456 | tf_op jit(solution)/shard_map/ppermute | solution.py:14
  117.7 0.0 collective-permute-done.2
  117.7 1.6 maximum_convert_fusion
  119.3 0.6 collective-permute-done.3
  119.9 1.6 maximum_convert_fusion.1
  121.5 64.6 %all-gather.5.cloned.1.call-done = bf16[704,2048]{0,1:T(8,128)(2,1)} async-done(((bf16[704,32]{0,1:T(8,128)(2,1)}), bf16[704,2048]{0,1:T(8,128)(2,1)}) %all-gather.5.cloned.1.call-update) | async-done | bytes 2883600 | tf_op jit(solution)/shard_map/all_gather | solution.py:144
  186.1 9.1 %convolution_convert_fusion.1 = bf16[512,2048]{1,0:T(8,128)(2,1)S(1)} fusion(bf16[704,2048]{0,1:T(8,128)(2,1)} %all-gather.5.cloned.1.call-done, f32[514,704]{0,1:T(8,128)} %maximum_convert_fusion.1, f32[514,704]{0,1:T(8,128)} %maximum_convert_fusion, f32[704]{0:T(1024)S(1)} %get-tuple-element.9, f32[704]{0:T(1024)S(1)} %get-tuple-element.10, ...), kind=kOutput, calls=%fused_computation.7 | convolution fusion | flops 1483210752 | bytes 13910528 | tf_op jit(solution)/shard_map/dot_general | solution.py:147
  195.2 34.6 %all_to_all.15 = bf16[8,64,2048]{2,1,0:T(8,128)(2,1)S(1)} all-to-all(bf16[8,64,2048]{2,1,0:T(8,128)(2,1)S(1)} %bitcast.47), channel_id=1, replica_groups=mesh['sp'=64,'tp'=8] {'tp'}, dimensions={0} | all-to-all | bytes 4194304 | tf_op jit(solution)/shard_map/all_to_all | solution.py:24
  229.8 0.4 convert_reduce_fusion
  230.1 0.1 multiply_reduce_fusion
  230.3 0.2 copy-done.5
  230.5 0.9 add_convert_fusion
  (20 shorter events, 0.2 us)
Async XLA Ops:
  6.5 16.4 %copy-start = (bf16[256,2048]{1,0:T(8,128)(2,1)S(1)}, bf16[256,2048]{1,0:T(8,128)(2,1)}, u32[]{:S(2)}) copy-start(bf16[256,2048]{1,0:T(8,128)(2,1)} %param.18) | copy-start | bytes 3145732
  6.5 14.6 %copy-start.2 = (bf16[512,64]{0,1:T(8,128)(2,1)S(1)}, bf16[512,64]{0,1:T(8,128)(2,1)}, u32[]{:S(2)}) copy-start(bf16[512,64]{0,1:T(8,128)(2,1)} %param.16) | copy-start | bytes 196612
  6.5 95.7 %all-gather.3.cloned.1.call-start = ((), (), s32[]{:S(2)}) async-start(), calls=%async_computation.3 | async-start | bytes 5857280 | tf_op jit(solution)/shard_map/all_gather | solution.py:46
  8.9 11.4 %collective-permute-start.1 = (bf16[128,64]{0,1:T(8,128)(2,1)S(1)}, bf16[128,64]{0,1:T(8,128)(2,1)S(1)}, u32[]{:S(2)}, u32[]{:S(2)}) collective-permute-start(bf16[128,64]{0,1:T(8,128)(2,1)S(1)} %slice.72), channel_id=1, source_target_pairs={{0,8},{8,16},{16,24},{24,32},{32,40},{40,48},{48,56},{56,64},{64,7... | collective-permute-start | bytes 49160 | tf_op jit(solution)/shard_map/ppermute | solution.py:14
  13.7 7.5 %collective-permute-start = (bf16[128,64]{0,1:T(8,128)(2,1)S(1)}, bf16[128,64]{0,1:T(8,128)(2,1)S(1)}, u32[]{:S(2)}, u32[]{:S(2)}) collective-permute-start(bf16[128,64]{0,1:T(8,128)(2,1)S(1)} %slice.68), channel_id=1, source_target_pairs={{0,8},{8,16},{16,24},{24,32},{32,40},{40,48},{48,56},{56,64},{64,7... | collective-permute-start | bytes 49160 | tf_op jit(solution)/shard_map/ppermute | solution.py:14
  20.2 1.5 copy-start.8
  25.1 32.8 %all-to-all-start = ((bf16[8,64,2048]{2,1,0:T(8,128)(2,1)}), bf16[8,64,2048]{2,1,0:T(8,128)(2,1)}, u32[]{:S(2)}, u32[]{:S(2)}) async-start(bf16[8,64,2048]{2,1,0:T(8,128)(2,1)} %bitcast.11), calls=%async_computation | async-start | bytes 4194304 | tf_op jit(solution)/shard_map/all_to_all | solution.py:24
  31.5 28.5 %copy-start.1 = (bf16[64,2048]{1,0:T(8,128)(2,1)S(1)}, bf16[64,2048]{1,0:T(8,128)(2,1)}, u32[]{:S(2)}) copy-start(bf16[64,2048]{1,0:T(8,128)(2,1)} %param.19) | copy-start | bytes 786436
  31.5 28.5 %copy-start.3 = (f32[2048]{0:T(1024)S(1)}, f32[2048]{0:T(1024)}, u32[]{:S(2)}) copy-start(f32[2048]{0:T(1024)} %param.20) | copy-start | bytes 24580
  31.5 28.8 %copy-start.4 = (f32[2048]{0:T(1024)S(1)}, f32[2048]{0:T(1024)}, u32[]{:S(2)}) copy-start(f32[2048]{0:T(1024)} %param.21) | copy-start | bytes 24580
  31.5 154.6 %all-gather.5.cloned.1.call-start = ((), (), s32[]{:S(2)}) async-start(), calls=%async_computation.4 | async-start | bytes 3194880 | tf_op jit(solution)/shard_map/all_gather | solution.py:144
  62.1 5.3 %copy-start.6 = (f32[3,704]{1,0:T(4,128)S(1)}, f32[3,704]{1,0:T(4,128)}, u32[]{:S(2)}) copy-start(f32[3,704]{1,0:T(4,128)} %param.26) | copy-start | bytes 25348
  62.1 5.3 %copy-start.7 = (f32[3,704]{1,0:T(4,128)S(1)}, f32[3,704]{1,0:T(4,128)}, u32[]{:S(2)}) copy-start(f32[3,704]{1,0:T(4,128)} %param.25) | copy-start | bytes 25348
  62.1 31.7 %all-to-all-start.1 = ((bf16[8,64,2048]{2,1,0:T(8,128)(2,1)}), bf16[8,64,2048]{2,1,0:T(8,128)(2,1)}, u32[]{:S(2)}, u32[]{:S(2)}) async-start(bf16[8,64,2048]{2,1,0:T(8,128)(2,1)} %broadcast_in_dim.16), calls=%async_computation.1 | async-start | bytes 4194304 | tf_op jit(solution)/shard_map/all_to_all | solution.py:36
  102.2 7.2 %copy-start.9 = (bf16[2048,1408]{1,0:T(8,128)(2,1)S(1)}, bf16[2048,1408]{1,0:T(8,128)(2,1)}, u32[]{:S(2)}) copy-start(bf16[2048,1408]{1,0:T(8,128)(2,1)} %all-gather.3.cloned.1.call-done) | copy-start | bytes 17301508
  106.7 11.0 %collective-permute-start.2 = (bf16[2,704]{0,1:T(8,128)(2,1)S(1)}, bf16[2,704]{0,1:T(8,128)(2,1)S(1)}, u32[]{:S(2)}, u32[]{:S(2)}) collective-permute-start(bf16[2,704]{0,1:T(8,128)(2,1)S(1)} %slice.90), channel_id=1, source_target_pairs={{0,8},{8,16},{16,24},{24,32},{32,40},{40,48},{48,56},{56,64},{64,7... | collective-permute-start | bytes 8456 | tf_op jit(solution)/shard_map/ppermute | solution.py:14
  114.0 5.9 %collective-permute-start.3 = (bf16[2,704]{0,1:T(8,128)(2,1)S(1)}, bf16[2,704]{0,1:T(8,128)(2,1)S(1)}, u32[]{:S(2)}, u32[]{:S(2)}) collective-permute-start(bf16[2,704]{0,1:T(8,128)(2,1)S(1)} %slice.94), channel_id=1, source_target_pairs={{0,8},{8,16},{16,24},{24,32},{32,40},{40,48},{48,56},{56,64},{64,7... | collective-permute-start | bytes 8456 | tf_op jit(solution)/shard_map/ppermute | solution.py:14
  229.8 0.7 copy-start.5
Sparse Core Ops, SparseCore 0:
  10.3 91.8 all-gather.2
  105.2 80.8 all-gather.4
where the time goes:
time: 239 us; the launch traced here: 238 us
  waiting for transfers between devices  126 us (53%)
  blocking collectives  34.6 us (14%)
  starting transfers between devices  25.4 us (11%)
  matrix products  21 us (9%)
  between operations  13.7 us (6%)
  other arithmetic  10.6 us (4%)
  local copies, waits for them, and re-layouts  6.82 us (3%)
    all_gather x1, waiting for transfers between devices, on_device(): down_whole = lax.all_gather(down_weight, 'sp', axis=1, tiled=True)  64.6 us
    all_to_all x1, blocking collectives, sum_at_owner(): lax.all_to_all(in_blocks(shard, dim, peers), axis, 0, 0, tiled=True)  34.6 us
    all_to_all x1, waiting for transfers between devices, sent_to_all(): return lax.all_to_all(copies, axis, split_axis=0, concat_axis=0, tiled=True)  26.3 us
    all_to_all x1, waiting for transfers between devices, sum_at_owner(): lax.all_to_all(in_blocks(shard, dim, peers), axis, 0, 0, tiled=True)  25.6 us
    ppermute x4, starting transfers between devices, passed_along(): return lax.ppermute(block, axis, route)  13.5 us
    dot_general x1, matrix products, on_device(): jnp.dot(selected, down_whole, preferred_element_type=jnp.float32)  9.1 us
    all_gather x1, waiting for transfers between devices, in_one_piece(): filled = lax.all_gather(both, axis, axis=dim, tiled=True)  8.4 us
    all_to_all x1, starting transfers between devices, sum_at_owner(): lax.all_to_all(in_blocks(shard, dim, peers), axis, 0, 0, tiled=True)  6.45 us
  transfers between devices with their start and end apart: 8, of which 5 were waited for; matrix products, arithmetic and copies ran while one was open for 11% of the time, Pallas kernels for 0%

commit v1 on v0

--- a/solution.py
+++ b/solution.py
@@ -141,7 +141,11 @@
     gate_conv = causal_local(gate_up, gate_before, gate_taps)
     value_conv = causal_local(value_up, value_before, value_taps)
     hidden = (jax.nn.silu(gate_conv) * value_conv).astype(jnp.bfloat16)
-    down_whole = lax.all_gather(down_weight, "sp", axis=1, tiled=True)
+    peers_2 = lax.axis_size("sp")
+    repeats = [peers_2 if d == 1 else 1 for d in range(down_weight.ndim)]
+    down_whole = lax.all_to_all(
+        jnp.tile(down_weight, repeats), "sp", split_axis=1, concat_axis=1, tiled=True
+    )
     selected = hidden
     down = sum_at_owner(
         jnp.dot(selected, down_whole, preferred_element_type=jnp.float32).astype(jnp.bfloat16),

time: 239 us -> 246 us (1.029)
  the two profiles are of different devices: /device:TPU:1 before, /device:TPU:80 now
where the time goes in v1:
time: 246 us; the launch traced here: 245 us
  blocking collectives  108 us (44%)
  waiting for transfers between devices  63.6 us (26%)
  starting transfers between devices  25 us (10%)
  matrix products  18.1 us (7%)
  between operations  13.7 us (6%)
  other arithmetic  8.84 us (4%)
  local copies, waits for them, and re-layouts  8.03 us (3%)
    all_to_all x2, blocking collectives, sum_at_owner(): lax.all_to_all(in_blocks(shard, dim, peers), axis, 0, 0, tiled=True)  77.5 us
    all_gather x1, waiting for transfers between devices, in_one_piece(): filled = lax.all_gather(both, axis, axis=dim, tiled=True)  33.5 us
    all_to_all x1, blocking collectives, sent_to_all(): return lax.all_to_all(copies, axis, split_axis=0, concat_axis=0, tiled=True)  30.5 us
    ppermute x4, waiting for transfers between devices, passed_along(): return lax.ppermute(block, axis, route)  30.1 us
    all_to_all x1, starting transfers between devices, on_device(): lax.all_to_all(jnp.tile(down_weight, repeats), 'sp', split_axis=1, concat...  12.8 us
    ppermute x4, starting transfers between devices, passed_along(): return lax.ppermute(block, axis, route)  12.2 us
    dot_general x1, matrix products, on_device(): jnp.dot(selected, down_whole, preferred_element_type=jnp.float32)  9.12 us
  transfers between devices with their start and end apart: 6, of which 3 were waited for; matrix products, arithmetic and copies ran while one was open for 9% of the time, Pallas kernels for 0%

profile of v1, /device:TPU:80, one launch (start us, length us, event | category | flops | bytes accessed | tf_op | source)
XLA Modules:
  0.0 245.4 jit_solution(11304663870542470977)
XLA Ops:
  6.5 0.0 copy-start
  6.5 0.0 copy-start.3
  6.5 0.0 all-gather.2.cloned.1.call-start
  6.5 0.8 slice.68
  7.4 3.5 %collective-permute-start = (bf16[128,64]{0,1:T(8,128)(2,1)S(1)}, bf16[128,64]{0,1:T(8,128)(2,1)S(1)}, u32[]{:S(2)}, u32[]{:S(2)}) collective-permute-start(bf16[128,64]{0,1:T(8,128)(2,1)S(1)} %slice.68), channel_id=1, source_target_pairs={{0,8},{8,16},{16,24},{24,32},{32,40},{40,48},{48,56},{56,64},{64,7... | collective-permute-start | bytes 49160 | tf_op jit(solution)/shard_map/ppermute | solution.py:14
  10.8 0.7 slice.72
  11.6 4.7 %collective-permute-start.1 = (bf16[128,64]{0,1:T(8,128)(2,1)S(1)}, bf16[128,64]{0,1:T(8,128)(2,1)S(1)}, u32[]{:S(2)}, u32[]{:S(2)}) collective-permute-start(bf16[128,64]{0,1:T(8,128)(2,1)S(1)} %slice.72), channel_id=1, source_target_pairs={{0,8},{8,16},{16,24},{24,32},{32,40},{40,48},{48,56},{56,64},{64,7... | collective-permute-start | bytes 49160 | tf_op jit(solution)/shard_map/ppermute | solution.py:14
  16.3 1.5 pad_maximum_fusion
  17.8 0.0 all-gather.2.cloned.1.call-update
  17.9 0.3 fusion.29
  18.2 0.9 slice.75
  19.1 0.9 slice.71
  20.0 0.0 copy-start.10
  20.0 1.2 reshape.143
  21.3 0.0 collective-permute-done.1
  21.3 0.8 pad_maximum_fusion.1
  22.1 0.0 collective-permute-done
  22.1 0.0 copy-done.3
  22.2 0.5 fusion.39
  22.7 0.0 copy-done.10
  22.7 0.1 broadcast_maximum_fusion
  22.8 0.3 fusion.4
  23.1 0.1 exponential_add_fusion
  23.2 0.5 fusion.17
  23.7 0.2 copy.25
  23.9 0.0 copy-done
  23.9 0.7 convolution_convert_fusion
  24.7 31.3 %all_to_all.24 = bf16[8,64,2048]{2,1,0:T(8,128)(2,1)S(1)} all-to-all(bf16[8,64,2048]{2,1,0:T(8,128)(2,1)S(1)} %bitcast.48), channel_id=1, replica_groups=mesh['sp'=64,'tp'=8] {'tp'}, dimensions={0} | all-to-all | bytes 4194304 | tf_op jit(solution)/shard_map/all_to_all | solution.py:24
  56.0 0.4 convert_reduce_fusion.1
  56.4 0.1 multiply_reduce_fusion.2
  56.5 0.4 copy-done.1
  57.0 0.0 copy-done.4
  57.0 0.3 multiply_reduce_fusion.1
  57.2 0.0 copy-done.6
  57.2 0.2 multiply_convert_fusion
  57.4 0.2 broadcast_in_dim.16
  57.7 0.0 copy-start.5
  57.7 30.5 %all_to_all.25 = bf16[8,64,2048]{2,1,0:T(8,128)(2,1)} all-to-all(bf16[8,64,2048]{2,1,0:T(8,128)(2,1)S(1)} %broadcast_in_dim.16), channel_id=1, replica_groups=mesh['sp'=64,'tp'=8] {'tp'}, dimensions={0} | all-to-all | bytes 4194304 | tf_op jit(solution)/shard_map/all_to_all | solution.py:36
  88.2 0.0 copy-done.5
  88.2 2.0 tile.2
  90.3 12.8 %all-to-all-start.2 = ((bf16[704,64,32]{0,2,1:T(8,128)(2,1)}), bf16[704,64,32]{0,2,1:T(8,128)(2,1)}, u32[]{:S(2)}, u32[]{:S(2)}) async-start(bf16[704,64,32]{0,2,1:T(8,128)(2,1)} %tile.2), calls=%async_computation.2 | async-start | bytes 6291456 | tf_op jit(solution)/shard_map/all_to_all | solution.py:146
  103.1 0.0 copy-done.8
  103.1 0.0 copy-done.9
  103.1 0.1 slice_reduce_fusion.2
  103.2 33.5 %all-gather.2.cloned.1.call-done = bf16[2048,1408]{1,0:T(8,128)(2,1)} async-done(((bf16[32,1408]{1,0:T(8,128)(2,1)}), bf16[2048,1408]{1,0:T(8,128)(2,1)}) %all-gather.2.cloned.1.call-update) | async-done | bytes 5767184 | tf_op jit(solution)/shard_map/all_gather | solution.py:46
  136.7 4.4 %fusion.11 = bf16[512,704]{0,1:T(8,128)(2,1)S(1)} fusion(bf16[512,2048]{1,0:T(8,128)(2,1)} %bitcast.49, bf16[2048,1408]{1,0:T(8,128)(2,1)} %all-gather.2.cloned.1.call-done), kind=kOutput, calls=%fused_computation.24 | convolution fusion | flops 1476755456 | bytes 5963776 | tf_op jit(solution)/shard_map/dot_general | solution.py:131
  141.1 0.1 slice.90
  141.2 1.9 collective-permute-start.2
  143.1 0.0 copy-done.2
  143.1 0.0 copy-done.11
  143.1 2.9 %fusion.14 = bf16[512,704]{0,1:T(8,128)(2,1)S(1)} fusion(bf16[512,2048]{1,0:T(8,128)(2,1)S(1)} %bitcast.50, bf16[2048,1408]{1,0:T(8,128)(2,1)S(1)} %copy-done.11), kind=kOutput, calls=%fused_computation.25 | convolution fusion | flops 1476755456 | bytes 5963776 | tf_op jit(solution)/shard_map/dot_general | solution.py:134
  146.0 0.1 slice.94
  146.1 2.1 collective-permute-start.3
  148.2 28.3 %collective-permute-done.2 = bf16[2,704]{0,1:T(8,128)(2,1)S(1)} collective-permute-done((bf16[2,704]{0,1:T(8,128)(2,1)S(1)}, bf16[2,704]{0,1:T(8,128)(2,1)S(1)}, u32[]{:S(2)}, u32[]{:S(2)}) %collective-permute-start.2) | collective-permute-done | bytes 2848 | tf_op jit(solution)/shard_map/ppermute | solution.py:14
  176.6 1.6 maximum_convert_fusion
  178.2 1.8 collective-permute-done.3
  180.0 1.6 maximum_convert_fusion.1
  181.6 0.0 all-to-all-done.2
  181.6 9.1 %convolution_convert_fusion.1 = bf16[512,2048]{1,0:T(8,128)(2,1)S(1)} fusion(bf16[704,2048]{0,1:T(8,128)(2,1)} %bitcast.13, f32[514,704]{0,1:T(8,128)} %maximum_convert_fusion.1, f32[514,704]{0,1:T(8,128)} %maximum_convert_fusion, f32[704]{0:T(1024)S(1)} %get-tuple-element.9, f32[704]{0:T(1024)S(1)} %get-tuple-element.10, f32[704]{0:T(1024)S(1)} %get-tuple-element.8, ...), kind=kOutput, calls=%fused_computation.7 | convolution fusion | flops 1483210752 | bytes 13910528 | tf_op jit(solution)/shard_map/dot_general | solution.py:151
  190.7 46.2 %all_to_all.26 = bf16[8,64,2048]{2,1,0:T(8,128)(2,1)S(1)} all-to-all(bf16[8,64,2048]{2,1,0:T(8,128)(2,1)S(1)} %bitcast.51), channel_id=1, replica_groups=mesh['sp'=64,'tp'=8] {'tp'}, dimensions={0} | all-to-all | bytes 4194304 | tf_op jit(solution)/shard_map/all_to_all | solution.py:24
  236.9 0.4 convert_reduce_fusion
  237.3 0.1 multiply_reduce_fusion
  237.4 0.2 copy-done.7
  237.6 0.9 add_convert_fusion
  (22 shorter events, 0.2 us)
Async XLA Ops:
  6.5 17.4 %copy-start = (bf16[256,2048]{1,0:T(8,128)(2,1)S(1)}, bf16[256,2048]{1,0:T(8,128)(2,1)}, u32[]{:S(2)}) copy-start(bf16[256,2048]{1,0:T(8,128)(2,1)} %param.18) | copy-start | bytes 3145732
  6.5 15.6 %copy-start.3 = (bf16[512,64]{0,1:T(8,128)(2,1)S(1)}, bf16[512,64]{0,1:T(8,128)(2,1)}, u32[]{:S(2)}) copy-start(bf16[512,64]{0,1:T(8,128)(2,1)} %param.16) | copy-start | bytes 196612
  6.5 130.1 %all-gather.2.cloned.1.call-start = ((), (), s32[]{:S(2)}) async-start(), calls=%async_computation.4 | async-start | bytes 5857280 | tf_op jit(solution)/shard_map/all_gather | solution.py:46
  7.4 14.8 %collective-permute-start = (bf16[128,64]{0,1:T(8,128)(2,1)S(1)}, bf16[128,64]{0,1:T(8,128)(2,1)S(1)}, u32[]{:S(2)}, u32[]{:S(2)}) collective-permute-start(bf16[128,64]{0,1:T(8,128)(2,1)S(1)} %slice.68), channel_id=1, source_target_pairs={{0,8},{8,16},{16,24},{24,32},{32,40},{40,48},{48,56},{56,64},{64,7... | collective-permute-start | bytes 49160 | tf_op jit(solution)/shard_map/ppermute | solution.py:14
  11.6 9.7 %collective-permute-start.1 = (bf16[128,64]{0,1:T(8,128)(2,1)S(1)}, bf16[128,64]{0,1:T(8,128)(2,1)S(1)}, u32[]{:S(2)}, u32[]{:S(2)}) collective-permute-start(bf16[128,64]{0,1:T(8,128)(2,1)S(1)} %slice.72), channel_id=1, source_target_pairs={{0,8},{8,16},{16,24},{24,32},{32,40},{40,48},{48,56},{56,64},{64,7... | collective-permute-start | bytes 49160 | tf_op jit(solution)/shard_map/ppermute | solution.py:14
  20.0 2.7 %copy-start.10 = (f32[4]{0:T(128)S(1)}, f32[4]{0:T(128)}, u32[]{:S(2)}) copy-start(f32[4]{0:T(128)} %param.17) | copy-start | bytes 52
  56.0 1.0 copy-start.1
  56.0 1.0 copy-start.4
  56.0 1.2 copy-start.6
  57.7 30.5 %copy-start.5 = (bf16[704,32]{0,1:T(8,128)(2,1)S(1)}, bf16[704,32]{0,1:T(8,128)(2,1)}, u32[]{:S(2)}) copy-start(bf16[704,32]{0,1:T(8,128)(2,1)} %param.27) | copy-start | bytes 135172
  90.3 12.9 %copy-start.8 = (f32[3,704]{1,0:T(4,128)S(1)}, f32[3,704]{1,0:T(4,128)}, u32[]{:S(2)}) copy-start(f32[3,704]{1,0:T(4,128)} %param.26) | copy-start | bytes 25348
  90.3 12.9 %copy-start.9 = (f32[3,704]{1,0:T(4,128)S(1)}, f32[3,704]{1,0:T(4,128)}, u32[]{:S(2)}) copy-start(f32[3,704]{1,0:T(4,128)} %param.25) | copy-start | bytes 25348
  90.3 91.3 %all-to-all-start.2 = ((bf16[704,64,32]{0,2,1:T(8,128)(2,1)}), bf16[704,64,32]{0,2,1:T(8,128)(2,1)}, u32[]{:S(2)}, u32[]{:S(2)}) async-start(bf16[704,64,32]{0,2,1:T(8,128)(2,1)} %tile.2), calls=%async_computation.2 | async-start | bytes 6291456 | tf_op jit(solution)/shard_map/all_to_all | solution.py:146
  136.7 6.4 %copy-start.2 = (bf16[8,64,2048]{2,1,0:T(8,128)(2,1)S(1)}, bf16[8,64,2048]{2,1,0:T(8,128)(2,1)}, u32[]{:S(2)}) copy-start(bf16[8,64,2048]{2,1,0:T(8,128)(2,1)} %all_to_all.25) | copy-start | bytes 6291460
  136.7 6.4 %copy-start.11 = (bf16[2048,1408]{1,0:T(8,128)(2,1)S(1)}, bf16[2048,1408]{1,0:T(8,128)(2,1)}, u32[]{:S(2)}) copy-start(bf16[2048,1408]{1,0:T(8,128)(2,1)} %all-gather.2.cloned.1.call-done) | copy-start | bytes 17301508
  141.2 35.4 %collective-permute-start.2 = (bf16[2,704]{0,1:T(8,128)(2,1)S(1)}, bf16[2,704]{0,1:T(8,128)(2,1)S(1)}, u32[]{:S(2)}, u32[]{:S(2)}) collective-permute-start(bf16[2,704]{0,1:T(8,128)(2,1)S(1)} %slice.90), channel_id=1, source_target_pairs={{0,8},{8,16},{16,24},{24,32},{32,40},{40,48},{48,56},{56,64},{64,7... | collective-permute-start | bytes 8456 | tf_op jit(solution)/shard_map/ppermute | solution.py:14
  146.1 33.8 %collective-permute-start.3 = (bf16[2,704]{0,1:T(8,128)(2,1)S(1)}, bf16[2,704]{0,1:T(8,128)(2,1)S(1)}, u32[]{:S(2)}, u32[]{:S(2)}) collective-permute-start(bf16[2,704]{0,1:T(8,128)(2,1)S(1)} %slice.94), channel_id=1, source_target_pairs={{0,8},{8,16},{16,24},{24,32},{32,40},{40,48},{48,56},{56,64},{64,7... | collective-permute-start | bytes 8456 | tf_op jit(solution)/shard_map/ppermute | solution.py:14
  236.9 0.7 copy-start.7
Sparse Core Ops, SparseCore 0:
  17.9 118.6 all-gather.1
